TPU v7x, 32 devices: a whole 2x2x4 slice. The times are simulated.
32 devices in a mesh: sp: 16 (over z, y, x), tp: 2 (over core).
Axes of the slice: x: 2, y: 2, z: 4, core: 2. Of those that a mesh axis runs over, the one named last changes fastest.
Arguments:
- queries: bfloat16 [2048, 1024], P('sp', 'tp'), may hold values from -6 to 6
- keys: bfloat16 [2048, 1024], P('sp', 'tp'), may hold values from -6 to 6
- values: bfloat16 [2048, 2048], P('sp', 'tp'), may hold values from -6 to 6
- out_gate: bfloat16 [2048, 2048], P('sp', 'tp'), may hold values from -6 to 6
- decay_rate: float32 [8], P('tp'), may hold values from 0 to 1
- residual: bfloat16 [2048, 2048], P(('sp', 'tp')), may hold values from -6 to 6
- out_weight: bfloat16 [2048, 2048], P('tp'), may hold values from -0.125 to 0.125
- ffn_gain: float32 [2048], replicated, may hold values from 0.1 to 1.9
- route_ids: int32 [2048, 4], P(('sp', 'tp')), may hold values from 0 to 15, all different within a row; in each aligned block of 64 rows (0 to 63, 64 to 127, ...) at most 32 rows name the same one
- route_weights: float32 [2048, 4], P(('sp', 'tp')), may hold values from 0.1 to 1
- gate_up: bfloat16 [16, 2048, 2048], P('sp', None, 'tp'), may hold values from -0.375 to 0.375
- lin_up: bfloat16 [16, 2048, 2048], P('sp', None, 'tp'), may hold values from -0.375 to 0.375
- down_weight: bfloat16 [16, 2048, 2048], P('sp', 'tp'), may hold values from -0.03125 to 0.03125
Outputs:
- layer_out: bfloat16 [2048, 2048], P(('sp', 'tp'))
Inputs may be any that keep to these rules, and one draw needn't show every extreme that they name: `route_ids`: within the rows of one device (aligned blocks of 64 rows), no expert is named by more than 32 entries, a bound that some block reaches; the 4 experts of a row differ.
All inputs are finite; a program needn't handle non-finite values.
Results may differ from a plain program's by a relative error of at most 0.03.
Values may be sent and summed in bfloat16 or wider, within the bound.
A program may use at most 128 MiB of HBM per device.

v0:
```python
import jax
import jax.numpy as jnp
from jax import lax
from jax.sharding import PartitionSpec as P

D = 2048
DK = 128
DV = 256


EPS = 1e-05
CLAMP_LIMIT = 7.0
SIGMOID_SLOPE = 1.702
TOP_PRECISION = lax.Precision.HIGHEST


def entering(array, axis, combine, identity):
    peers, mine = (lax.axis_size(axis), lax.axis_index(axis))
    everything = jax.tree.map(
        lambda part, kind: lax.all_gather(part.astype(kind), axis),
        array,
        (jnp.bfloat16, jnp.bfloat16),
    )
    start = jax.tree.map(
        lambda part, zero: jnp.broadcast_to(jnp.asarray(zero, part.dtype), part.shape),
        array,
        identity,
    )

    def turn(k, before):
        reached = k < mine
        new = combine(
            before, jax.tree.map(lambda part, own: part[k].astype(own.dtype), everything, array)
        )
        return jax.tree.map(lambda a, b: jnp.where(reached, a, b), new, before)

    return lax.fori_loop(0, peers, turn, start)


def expert_act(row_block, gate_part, lin_part):
    gate_pre = jnp.dot(row_block, gate_part, preferred_element_type=jnp.float32)
    lin_pre = jnp.dot(row_block, lin_part, preferred_element_type=jnp.float32)
    gate_clip = jnp.minimum(gate_pre, CLAMP_LIMIT)
    lin_clip = jnp.clip(lin_pre, -CLAMP_LIMIT, CLAMP_LIMIT)
    return (gate_clip * jax.nn.sigmoid(SIGMOID_SLOPE * gate_clip) * (lin_clip + 1.0)).astype(
        jnp.bfloat16
    )


def combine_state(before_part, after_part):
    return (
        before_part[0] * after_part[0],
        after_part[0][:, None, None] * before_part[1] + after_part[1],
    )


def local(
    queries,
    keys,
    values,
    out_gate,
    decay_rate,
    residual,
    out_weight,
    ffn_gain,
    route_ids,
    route_weights,
    gate_up,
    lin_up,
    down_weight,
):
    block_len = queries.shape[0]
    local_heads = decay_rate.shape[0]
    log_gamma = -decay_rate
    query_heads = queries.astype(jnp.float32).reshape(block_len, local_heads, DK).transpose(1, 0, 2)
    per_head_keys = keys.astype(jnp.float32).reshape(block_len, local_heads, DK).transpose(
        1, 0, 2
    ) * DK ** (-0.5)
    per_head_values = (
        values.astype(jnp.float32).reshape(block_len, local_heads, DV).transpose(1, 0, 2)
    )
    positions = jnp.arange(block_len, dtype=jnp.float32)
    offsets = positions[:, None] - positions[None, :]
    causal = offsets >= 0
    decay_mask = jnp.where(
        causal[None], jnp.exp(jnp.where(causal, offsets, 0.0)[None] * log_gamma[:, None, None]), 0.0
    )
    trailing_decay = jnp.exp((block_len - 1.0 - positions)[None, :] * log_gamma[:, None])
    lead_decay = jnp.exp((positions + 1.0)[None, :] * log_gamma[:, None])
    chain_decay = jnp.exp(block_len * log_gamma)
    attention_scores = (
        jnp.einsum("hqd,hkd->hqk", query_heads, per_head_keys, precision=TOP_PRECISION) * decay_mask
    )
    intra_block_term = jnp.einsum(
        "zfp,zpn->zfn", attention_scores, per_head_values, precision=TOP_PRECISION
    )
    state_delta = jnp.einsum(
        "mxs,mxq->msq",
        per_head_keys * trailing_decay[:, :, None],
        per_head_values,
        precision=TOP_PRECISION,
    )
    identity = (jnp.ones_like(chain_decay), jnp.zeros_like(state_delta))
    carried = entering((chain_decay, state_delta), "sp", combine_state, identity)[1]
    cross_term = (
        jnp.einsum("hqd,hdv->hqv", query_heads, carried, precision=TOP_PRECISION)
        * lead_decay[:, :, None]
    )
    retained = intra_block_term + cross_term
    normed = retained * lax.rsqrt(jnp.mean(retained * retained, axis=-1, keepdims=True) + EPS)
    gated = (
        normed.transpose(1, 0, 2).reshape(block_len, local_heads * DV)
        * jax.nn.silu(out_gate.astype(jnp.float32))
    ).astype(jnp.bfloat16)
    mix_rows = lax.psum_scatter(
        jnp.dot(gated, out_weight, preferred_element_type=jnp.float32).astype(jnp.bfloat16),
        "tp",
        scatter_dimension=0,
        tiled=True,
    ).astype(jnp.float32)
    mixed = (residual.astype(jnp.float32) + mix_rows).astype(jnp.bfloat16)
    mixed_wide = mixed.astype(jnp.float32)
    normed_rows = (
        mixed_wide
        * lax.rsqrt(jnp.mean(mixed_wide * mixed_wide, axis=-1, keepdims=True) + EPS)
        * ffn_gain
    ).astype(jnp.bfloat16)
    experts = lax.axis_size("sp")
    own_rows = route_ids.shape[0]
    top_count = route_ids.shape[1]
    capacity = own_rows * top_count * lax.axis_size("tp") // experts
    flat_ids = route_ids.reshape(-1)
    one_hot = (flat_ids[:, None] == jnp.arange(experts, dtype=jnp.int32)[None, :]).astype(jnp.int32)
    slot_rank = jnp.sum(one_hot * (jnp.cumsum(one_hot, axis=0) - 1), axis=1)
    slot_index = flat_ids * capacity + slot_rank
    source_row = jnp.arange(own_rows * top_count, dtype=jnp.int32) // top_count
    slot_source = (
        jnp.full((experts * capacity,), own_rows, jnp.int32).at[slot_index].set(source_row)
    )
    padded = jnp.concatenate([normed_rows, jnp.zeros((1, D), jnp.bfloat16)], axis=0)
    outgoing = padded[slot_source].reshape(experts, capacity, D)
    gate_half = gate_up[0]
    lin_half = lin_up[0]
    down_half = down_weight[0]
    pair_rows = lax.all_gather(
        lax.all_to_all(outgoing, "sp", split_axis=0, concat_axis=0, tiled=True),
        "tp",
        axis=0,
        tiled=True,
    )
    activation = expert_act(pair_rows.reshape(-1, D), gate_half, lin_half)
    partial_value = jnp.dot(activation, down_half, preferred_element_type=jnp.float32).reshape(
        pair_rows.shape
    )
    summed = lax.psum_scatter(
        partial_value.astype(jnp.bfloat16), "tp", scatter_dimension=0, tiled=True
    )
    returned = lax.all_to_all(summed, "sp", split_axis=0, concat_axis=0, tiled=True)
    picked = (
        returned.reshape(experts * capacity, D)[slot_index]
        .reshape(own_rows, top_count, D)
        .astype(jnp.float32)
    )
    expert_sum = jnp.sum(picked * route_weights[:, :, None], axis=1)
    return (mixed_wide + expert_sum).astype(jnp.bfloat16)


def solution(mesh):
    placed = (
        P("sp", "tp"),
        P("sp", "tp"),
        P("sp", "tp"),
        P("sp", "tp"),
        P("tp"),
        P(("sp", "tp"), None),
        P("tp", None),
        P(),
        P(("sp", "tp"), None),
        P(("sp", "tp"), None),
        P("sp", None, "tp"),
        P("sp", None, "tp"),
        P("sp", "tp", None),
    )
    return jax.shard_map(
        local, mesh=mesh, in_specs=placed, out_specs=P(("sp", "tp"), None), check_vma=False
    )
```

profile of v0, /device:TPU:0, one launch (start us, length us, event | category | flops | bytes accessed | tf_op | source)
XLA Modules:
  0.0 287.8 jit_solution(7690328628318113255)
XLA Ops:
  6.5 0.7 fusion.44
  7.2 1.0 copy.53
  8.3 0.1 multiply_exponential_fusion
  8.3 2.0 convolution_convert_fusion.1
  10.4 0.0 reduce-scatter.3.cloned.1.call-start
  10.4 1.3 dynamic-slice
  12.3 0.2 dynamic-update-slice
  12.6 43.9 %all-reduce.1 = bf16[64]{0:T(256)(128)(2,1)S(1)} all-reduce(bf16[64]{0:T(256)(128)(2,1)S(1)} %dynamic-update-slice), channel_id=2, replica_groups=mesh['sp'=16,'tp'=2] {'sp'}, use_global_device_ids=true, to_apply=%add.1 | all-reduce | flops 64 | bytes 256
  56.5 0.1 reshape.228
  56.6 1.1 copy.43
  57.7 0.8 copy.45
  58.5 0.1 eq.29
  58.6 0.6 reduce-window.6
  59.3 0.1 multiply_exponential_fusion.1
  59.4 0.4 fusion.12
  59.8 29.2 %all-gather.7.cloned.1.call-done = bf16[64,128,256]{2,1,0:T(8,128)(2,1)} async-done(((bf16[4,128,256]{2,1,0:T(8,128)(2,1)}), bf16[64,128,256]{2,1,0:T(8,128)(2,1)}) %all-gather.7.cloned.1.call-update) | async-done | bytes 4194320 | tf_op jit(solution)/shard_map/all_gather | solution.py:20
  89.0 18.1 %while.14 = (s32[]{:T(128)}, f32[4,128,256]{2,1,0:T(8,128)S(1)}, s32[]{:T(128)}, bf16[16,4]{1,0:T(8,128)(2,1)S(1)}, bf16[16,4,128,256]{3,2,1,0:T(8,128)(2,1)}, /*index=5*/s32[]{:T(128)}, s32[]{:T(128)}) while((s32[]{:T(128)}, f32[4,128,256]{2,1,0:T(8,128)S(1)}, s32[]{:T(128)}, bf16[16,4]{1,0:T(8,128)(2,1)S(1)}, ...), condition=%wide.region_1.2_spmd.clone, body=%wide.region_0.1_spmd.clone.sunk | while | flops 655368 | bytes 1310865 | solution.py:37
  89.0 1.1 fusion.55
  90.1 1.1 fusion.55
  91.2 1.1 fusion.55
  92.4 1.1 fusion.55
  93.5 1.1 fusion.55
  94.6 1.1 fusion.55
  95.8 1.1 fusion.55
  96.9 1.1 fusion.55
  98.0 1.1 fusion.55
  99.2 1.1 fusion.55
  100.3 1.1 fusion.55
  101.4 1.1 fusion.55
  102.6 1.1 fusion.55
  103.7 1.1 fusion.55
  104.8 1.1 fusion.55
  106.0 1.1 fusion.55
  107.1 0.4 fusion.31
  107.5 0.5 fusion.22
  108.0 0.2 fusion.24
  108.3 0.2 copy.42
  108.5 0.2 fusion.25
  108.6 3.7 %convolution_convert_fusion = bf16[128,2048]{1,0:T(8,128)(2,1)} fusion(bf16[128,1024]{0,1:T(8,128)(2,1)S(1)} %fusion.25, bf16[1024,2048]{1,0:T(8,128)(2,1)} %param.21), kind=kOutput, calls=%fused_computation.14 | convolution fusion | flops 537133056 | bytes 4980736 | tf_op jit(solution)/shard_map/dot_general | solution.py:116
  112.4 0.0 all-gather.5.cloned.1.call-start
  112.4 0.2 slice_reduce_fusion
  112.6 0.1 eq.25
  112.8 0.1 copy.44
  112.9 0.1 mul.227
  113.0 0.1 fusion.39
  113.1 1.4 scatter_custom_fusion
  114.5 4.5 %reduce-scatter.3.cloned.1.call-done = bf16[64,2048]{1,0:T(8,128)(2,1)} async-done(((bf16[128,2048]{1,0:T(8,128)(2,1)}), bf16[64,2048]{1,0:T(8,128)(2,1)}) %reduce-scatter.3.cloned.1.call-update) | async-done | bytes 262160 | tf_op jit(solution)/shard_map/reduce_scatter | solution.py:115
  119.1 1.1 fusion.17
  120.2 1.1 fusion.19
  121.3 2.5 gather_fusion
  123.8 55.8 %all_to_all.10 = bf16[16,32,2048]{2,1,0:T(8,128)(2,1)} all-to-all(bf16[16,32,2048]{2,1,0:T(8,128)(2,1)S(1)} %bitcast.110), channel_id=1, replica_groups=mesh['sp'=16,'tp'=2] {'sp'}, dimensions={0} | all-to-all | bytes 4194304 | tf_op jit(solution)/shard_map/all_to_all | solution.py:146
  179.7 0.2 reduce-scatter.5.cloned.1.call-start
  179.9 12.0 %all-gather.5.cloned.1.call-done = bf16[32,32,2048]{2,1,0:T(8,128)(2,1)} async-done(((bf16[16,32,2048]{2,1,0:T(8,128)(2,1)}), bf16[32,32,2048]{2,1,0:T(8,128)(2,1)}) %all-gather.5.cloned.1.call-update) | async-done | bytes 4194320 | tf_op jit(solution)/shard_map/all_gather | solution.py:145
  191.9 7.6 %fusion.3 = f32[1024,1024]{1,0:T(8,128)S(1)} fusion(bf16[1024,2048]{1,0:T(8,128)(2,1)} %bitcast.119, bf16[1,2048,1024]{2,1,0:T(8,128)(2,1)} %param.26), kind=kOutput, calls=%fused_computation.8 | convolution fusion | flops 4294967296 | bytes 12582912 | tf_op jit(solution)/shard_map/dot_general | solution.py:42
  199.6 5.7 %multiply_convert_fusion = bf16[1024,1024]{1,0:T(8,128)(2,1)S(1)} fusion(f32[1024,1024]{1,0:T(8,128)S(1)} %fusion.3, bf16[1024,2048]{1,0:T(8,128)(2,1)S(1)} %bitcast.120, bf16[1,2048,1024]{2,1,0:T(8,128)(2,1)S(1)} %copy-done.6), kind=kOutput, calls=%fused_computation.12 | convolution fusion | flops 4305453056 | bytes 14680064 | tf_op jit(solution)/shard_map/dot_general | solution.py:41
  205.4 6.1 %fusion.7 = bf16[32,32,2048]{2,1,0:T(8,128)(2,1)} fusion(bf16[32,32,1024]{2,1,0:T(8,128)(2,1)S(1)} %bitcast.121, bf16[1,1024,2048]{2,1,0:T(8,128)(2,1)S(1)} %copy-done.7), kind=kOutput, calls=%fused_computation.13 | convolution fusion | flops 4297064448 | bytes 10485760 | tf_op jit(solution)/shard_map/dot_general | solution.py:152
  211.5 13.4 %reduce-scatter.5.cloned.1.call-done = bf16[16,32,2048]{2,1,0:T(8,128)(2,1)} async-done(((bf16[32,32,2048]{2,1,0:T(8,128)(2,1)}), bf16[16,32,2048]{2,1,0:T(8,128)(2,1)}) %reduce-scatter.5.cloned.1.call-update) | async-done | bytes 2097168 | tf_op jit(solution)/shard_map/reduce_scatter | solution.py:155
  224.9 6.9 %all-to-all-start.1 = ((bf16[16,32,2048]{2,1,0:T(8,128)(2,1)}), bf16[16,32,2048]{2,1,0:T(8,128)(2,1)S(1)}, u32[]{:S(2)}, u32[]{:S(2)}) async-start(bf16[16,32,2048]{2,1,0:T(8,128)(2,1)} %reduce-scatter.5.cloned.1.call-done), calls=%async_computation.3 | async-start | bytes 4194304 | tf_op jit(solution)/shard_map/all_to_all | solution.py:158
  231.8 0.7 copy.48
  232.5 42.5 %all-to-all-done.1 = bf16[16,32,2048]{2,1,0:T(8,128)(2,1)S(1)} async-done(((bf16[16,32,2048]{2,1,0:T(8,128)(2,1)}), bf16[16,32,2048]{2,1,0:T(8,128)(2,1)S(1)}, u32[]{:S(2)}, u32[]{:S(2)}) %all-to-all-start.1) | async-done | bytes 2097184 | tf_op jit(solution)/shard_map/all_to_all | solution.py:158
  275.1 1.4 gather_fusion.1
  276.4 0.7 reshape.202
  277.1 2.4 multiply_reduce_fusion
  279.5 1.8 fusion.20
  (56 shorter events, 0.5 us)
Async XLA Ops:
  6.5 52.8 %copy-start = (bf16[128,512]{1,0:T(8,128)(2,1)S(1)}, bf16[128,512]{1,0:T(8,128)(2,1)}, u32[]{:S(2)}) copy-start(bf16[128,512]{1,0:T(8,128)(2,1)} %param.15) | copy-start | bytes 393220
  6.5 82.4 %all-gather.7.cloned.1.call-start = ((), (), s32[]{:S(2)}) async-start(), calls=%async_computation.7 | async-start | bytes 4456448 | tf_op jit(solution)/shard_map/all_gather | solution.py:20
  10.4 108.7 %reduce-scatter.3.cloned.1.call-start = ((), (), s32[]{:S(2)}) async-start(), calls=%async_computation.4 | async-start | bytes 786432 | tf_op jit(solution)/shard_map/reduce_scatter | solution.py:115
  59.4 48.1 %copy-start.2 = (bf16[128,1024]{1,0:T(8,128)(2,1)S(1)}, bf16[128,1024]{1,0:T(8,128)(2,1)}, u32[]{:S(2)}) copy-start(bf16[128,1024]{1,0:T(8,128)(2,1)} %param.17) | copy-start | bytes 786436
  108.2 4.5 %copy-start.4 = (s32[64,4]{0,1:T(4,128)S(1)}, s32[64,4]{0,1:T(4,128)}, u32[]{:S(2)}) copy-start(s32[64,4]{0,1:T(4,128)} %param.23) | copy-start | bytes 3076
  108.2 10.8 %copy-start.1 = (bf16[64,2048]{1,0:T(8,128)(2,1)S(1)}, bf16[64,2048]{1,0:T(8,128)(2,1)}, u32[]{:S(2)}) copy-start(bf16[64,2048]{1,0:T(8,128)(2,1)} %param.20) | copy-start | bytes 786436
  108.3 11.9 %copy-start.3 = (f32[2048]{0:T(1024)S(1)}, f32[2048]{0:T(1024)}, u32[]{:S(2)}) copy-start(f32[2048]{0:T(1024)} %param.22) | copy-start | bytes 24580
  112.4 79.5 %all-gather.5.cloned.1.call-start = ((), (), s32[]{:S(2)}) async-start(), calls=%async_computation.5 | async-start | bytes 6291456 | tf_op jit(solution)/shard_map/all_gather | solution.py:145
  179.7 45.2 %reduce-scatter.5.cloned.1.call-start = ((), (), s32[]{:S(2)}) async-start(), calls=%async_computation.6 | async-start | bytes 6291456 | tf_op jit(solution)/shard_map/reduce_scatter | solution.py:155
  191.9 7.7 %copy-start.6 = (bf16[1,2048,1024]{2,1,0:T(8,128)(2,1)S(1)}, bf16[1,2048,1024]{2,1,0:T(8,128)(2,1)}, u32[]{:S(2)}) copy-start(bf16[1,2048,1024]{2,1,0:T(8,128)(2,1)} %param.25) | copy-start | bytes 12582916
  191.9 7.7 %copy-start.8 = (bf16[32,32,2048]{2,1,0:T(8,128)(2,1)S(1)}, bf16[32,32,2048]{2,1,0:T(8,128)(2,1)}, u32[]{:S(2)}) copy-start(bf16[32,32,2048]{2,1,0:T(8,128)(2,1)} %all-gather.5.cloned.1.call-done) | copy-start | bytes 12582916
  199.6 5.8 %copy-start.7 = (bf16[1,1024,2048]{2,1,0:T(8,128)(2,1)S(1)}, bf16[1,1024,2048]{2,1,0:T(8,128)(2,1)}, u32[]{:S(2)}) copy-start(bf16[1,1024,2048]{2,1,0:T(8,128)(2,1)} %param.27) | copy-start | bytes 12582916
  211.5 20.3 %copy-start.5 = (f32[64,4]{0,1:T(4,128)S(1)}, f32[64,4]{0,1:T(4,128)}, u32[]{:S(2)}) copy-start(f32[64,4]{0,1:T(4,128)} %param.24) | copy-start | bytes 3076
  224.9 50.2 %all-to-all-start.1 = ((bf16[16,32,2048]{2,1,0:T(8,128)(2,1)}), bf16[16,32,2048]{2,1,0:T(8,128)(2,1)S(1)}, u32[]{:S(2)}, u32[]{:S(2)}) async-start(bf16[16,32,2048]{2,1,0:T(8,128)(2,1)} %reduce-scatter.5.cloned.1.call-done), calls=%async_computation.3 | async-start | bytes 4194304 | tf_op jit(solution)/shard_map/all_to_all | solution.py:158
Sparse Core Ops, SparseCore 0:
  10.5 78.4 all-gather.6
  112.5 6.5 reduce-scatter.2
  179.8 12.0 all-gather.4
  211.6 13.2 reduce-scatter.4
where the time goes:
time: 293 us; the launch traced here: 288 us
  waiting for transfers between devices  102 us (35%)
  blocking collectives  99.8 us (34%)
  matrix products  26.6 us (9%)
  other arithmetic  26 us (9%)
  between operations  14.1 us (5%)
  local copies, waits for them, and re-layouts  12 us (4%)
  starting transfers between devices  7.21 us (2%)
    all_to_all x1, blocking collectives, local(): lax.all_to_all(outgoing, 'sp', split_axis=0, concat_axis=0, tiled=True)  55.8 us
    unnamed x1, blocking collectives  43.9 us
    all_to_all x1, waiting for transfers between devices, local(): lax.all_to_all(summed, 'sp', split_axis=0, concat_axis=0, tiled=True)  42.5 us
    all_gather x1, waiting for transfers between devices, entering(): lax.all_gather(part.astype(kind), axis)  29.2 us
    select_n x16, other arithmetic, turn(): return jax.tree.map(lambda a, b: jnp.where(reached, a, b), new, before)  17.5 us
    reduce_scatter x1, waiting for transfers between devices, local(): lax.psum_scatter(partial_value.astype(jnp.bfloat16), 'tp', scatter_dimens...  13.4 us
    all_gather x1, waiting for transfers between devices, local(): lax.all_gather(lax.all_to_all(outgoing, 'sp', split_axis=0, concat_axis=0...  12 us
    dot_general x1, matrix products, expert_act(): lin_pre = jnp.dot(row_block, lin_part, preferred_element_type=jnp.float32)  7.65 us
  transfers between devices with their start and end apart: 5, of which 5 were waited for; matrix products, arithmetic and copies ran while one was open for 3% of the time, Pallas kernels for 0%

commit v1 on v0

v1 whole, which is shorter than its diff:
```python
import functools

import jax
import jax.numpy as jnp
from jax import lax
from jax.experimental import pallas as pl
from jax.experimental.pallas import tpu as pltpu
from jax.sharding import PartitionSpec as P

D = 2048
DK = 128
DV = 256


EPS = 1e-05
CLAMP_LIMIT = 7.0
SIGMOID_SLOPE = 1.702
TOP_PRECISION = lax.Precision.HIGHEST


COLUMN = 4
MESH = pl.DeviceIdType.MESH
VMEM = pl.BlockSpec(memory_space=pltpu.VMEM)
ANY = pl.BlockSpec(memory_space=pl.ANY)
DMA = pltpu.SemaphoreType.DMA


def push(src, dst, send, recv, sp, tp):
    return pltpu.make_async_remote_copy(
        src_ref=src,
        dst_ref=dst,
        send_sem=send,
        recv_sem=recv,
        device_id=(sp, tp),
        device_id_type=MESH,
    )


def greet(devices):
    barrier = pltpu.get_barrier_semaphore()
    for sp, tp in devices:
        pl.semaphore_signal(barrier, inc=1, device_id=(sp, tp), device_id_type=MESH)
    pl.semaphore_wait(barrier, len(devices))


def state_kernel(n, delta, decay, carried, inbox, outbox, send1, recv1, send2, recv2):
    me, core = lax.axis_index("sp"), lax.axis_index("tp")
    greet([(lax.rem(me + k, n), core) for k in range(1, n)])

    def out_copy(k):
        to = lax.rem(me + k, n)
        return push(delta.at[to], inbox.at[me], send1.at[k], recv1.at[k], to, core)

    def in_copy(k):
        frm = lax.rem(me + n - k, n)
        return push(delta.at[me], inbox.at[frm], send1.at[k], recv1.at[k], frm, core)

    def back_out(k):
        to = lax.rem(me + k, n)
        return push(outbox.at[to], carried.at[me], send2.at[k], recv2.at[k], to, core)

    def back_in(k):
        frm = lax.rem(me + n - k, n)
        return push(outbox.at[me], carried.at[frm], send2.at[k], recv2.at[k], frm, core)

    def each(act):
        lax.fori_loop(1, n, lambda k, c: (act(k), c)[1], 0)

    each(lambda k: out_copy(k).start())
    inbox[me] = delta[me]
    each(lambda k: in_copy(k).wait_recv())
    factor = decay[...]

    def step(s, total):
        outbox[s] = total.astype(jnp.bfloat16)
        return factor * total + inbox[s].astype(jnp.float32)

    lax.fori_loop(0, n, step, jnp.zeros(factor.shape, jnp.float32))
    each(lambda k: back_out(k).start())
    carried[me] = outbox[me]
    each(lambda k: back_in(k).wait_recv())
    each(lambda k: out_copy(k).wait_send())
    each(lambda k: back_out(k).wait_send())


def exchange_states(delta, decay):
    n = delta.shape[0]
    return pl.pallas_call(
        functools.partial(state_kernel, n),
        out_shape=jax.ShapeDtypeStruct(delta.shape, jnp.bfloat16),
        in_specs=[VMEM, VMEM],
        out_specs=VMEM,
        scratch_shapes=[
            pltpu.VMEM(delta.shape, jnp.bfloat16),
            pltpu.VMEM(delta.shape, jnp.bfloat16),
            DMA((n,)),
            DMA((n,)),
            DMA((n,)),
            DMA((n,)),
        ],
        compiler_params=pltpu.CompilerParams(collective_id=0, has_side_effects=True),
        name="states",
    )(delta, decay)


def partners(nz, np_):
    me, core = lax.axis_index("sp"), lax.axis_index("tp")
    z, p = me // np_, lax.rem(me, np_)
    devices = [(me, 1 - core)]
    devices += [((z ^ d) * np_ + p, core) for d in range(1, nz)]
    devices += [(z * np_ + (p ^ k), core) for k in range(1, np_)]
    return me, core, z, p, devices


def dispatch_kernel(
    nz,
    np_,
    part,
    residual,
    gain,
    picks,
    weights,
    mixed,
    landed,
    weights_in,
    part_in,
    rows,
    picks_in,
    stage,
    part_sem,
    row_send,
    row_recv,
    pick_send,
    pick_recv,
    weight_send,
    weight_recv,
    plane_send,
    plane_recv,
    core_send,
    core_recv,
    own_sem,
):
    me, core, z, p, devices = partners(nz, np_)
    other = 1 - core
    own_rows = residual.shape[0]
    cap = landed.shape[3]
    greet(devices)

    def half(which):
        return part.at[pl.ds(pl.multiple_of(which * own_rows, own_rows), own_rows)]

    swap = push(half(other), part_in, part_sem.at[0], part_sem.at[1], me, other)
    swap.start()

    def column(d, kind):
        there = z ^ d
        to = there * np_ + p
        if kind == "pick":
            return push(
                picks.at[there], picks_in.at[z], pick_send.at[d], pick_recv.at[d], to, core
            )
        if kind == "weight":
            return push(
                weights.at[there], weights_in.at[z], weight_send.at[d], weight_recv.at[d], to, core
            )
        return push(rows.at[z], rows.at[z], row_send.at[d], row_recv.at[d], to, core)

    def column_in(d, kind):
        there = z ^ d
        to = there * np_ + p
        if kind == "pick":
            return push(
                picks.at[z], picks_in.at[there], pick_send.at[d], pick_recv.at[d], to, core
            )
        if kind == "weight":
            return push(
                weights.at[z], weights_in.at[there], weight_send.at[d], weight_recv.at[d], to, core
            )
        return push(rows.at[there], rows.at[there], row_send.at[d], row_recv.at[d], to, core)

    for d in range(1, nz):
        column(d, "pick").start()
    picks_in[z] = picks[z]
    weights_in[z] = weights[z]
    swap.wait_recv()
    wide = residual[...].astype(jnp.float32) + (
        half(core)[...].astype(jnp.float32) + part_in[...].astype(jnp.float32)
    )
    mixed[...] = wide.astype(jnp.bfloat16)
    wide = mixed[...].astype(jnp.float32)
    scale = lax.rsqrt(jnp.mean(wide * wide, axis=-1, keepdims=True) + EPS)
    rows[z] = (wide * scale * gain[...]).astype(jnp.bfloat16)
    for d in range(1, nz):
        column(d, "row").start()
    for d in range(1, nz):
        column(d, "weight").start()

    def plane(d, k):
        q = p ^ k
        src = stage.at[z ^ d, pl.ds(pl.multiple_of(q * cap, cap), cap)]
        return push(
            src,
            landed.at[p, z ^ d, core],
            plane_send.at[d, k],
            plane_recv.at[d, k],
            z * np_ + q,
            core,
        )

    def plane_in(d, k):
        q = p ^ k
        src = stage.at[z ^ d, pl.ds(pl.multiple_of(q * cap, cap), cap)]
        return push(
            src,
            landed.at[q, z ^ d, core],
            plane_send.at[d, k],
            plane_recv.at[d, k],
            z * np_ + q,
            core,
        )

    def own(d):
        src = stage.at[z ^ d, pl.ds(pl.multiple_of(p * cap, cap), cap)]
        return pltpu.make_async_copy(src, landed.at[p, z ^ d, core], own_sem.at[d])

    def forward(d, k):
        where = landed.at[p ^ k, z ^ d, core]
        return push(where, where, core_send.at[d, k], core_recv.at[d, k], me, other)

    def forward_own(d):
        src = stage.at[z ^ d, pl.ds(pl.multiple_of(p * cap, cap), cap)]
        return push(
            src, landed.at[p, z ^ d, core], core_send.at[d, 0], core_recv.at[d, 0], me, other
        )

    def forward_in(d, k):
        where = landed.at[p ^ k, z ^ d, other]
        return push(where, where, core_send.at[d, k], core_recv.at[d, k], me, other)

    def each(first, act):
        lax.fori_loop(first, np_, lambda k, c: (act(k), c)[1], 0)

    width = min(512, D)
    for d in range(nz):
        if d:
            column_in(d, "pick").wait_recv()
            column_in(d, "row").wait_recv()
        there = z ^ d
        for start in range(0, D, width):
            stage[there, :, start : start + width] = jnp.dot(
                picks_in[there],
                rows[there, :, start : start + width],
                preferred_element_type=jnp.float32,
            ).astype(jnp.bfloat16)
        each(1, lambda k: plane(d, k).start())
        own(d).start()
        forward_own(d).start()
    for d in range(nz):

        def pass_on(k):
            plane_in(d, k).wait_recv()
            forward(d, k).start()

        each(1, pass_on)
    for d in range(nz):
        each(0, lambda k: forward_in(d, k).wait_recv())
        own(d).wait()
        if d:
            column_in(d, "weight").wait_recv()
    swap.wait_send()
    for d in range(nz):
        if d:
            for kind in ("pick", "row", "weight"):
                column(d, kind).wait_send()
        each(1, lambda k: plane(d, k).wait_send())
        forward_own(d).wait_send()
        each(1, lambda k: forward(d, k).wait_send())


def dispatch(part, residual, gain, picks, weights, np_, cap):
    nz = picks.shape[0]
    own_rows, width = residual.shape
    return pl.pallas_call(
        functools.partial(dispatch_kernel, nz, np_),
        out_shape=(
            jax.ShapeDtypeStruct(residual.shape, jnp.bfloat16),
            jax.ShapeDtypeStruct((np_, nz, 2, cap, width), jnp.bfloat16),
            jax.ShapeDtypeStruct(weights.shape, jnp.bfloat16),
        ),
        in_specs=[VMEM] * 5,
        out_specs=(VMEM, ANY, VMEM),
        scratch_shapes=[
            pltpu.VMEM(residual.shape, jnp.bfloat16),
            pltpu.VMEM((nz, own_rows, width), jnp.bfloat16),
            pltpu.VMEM(picks.shape, jnp.bfloat16),
            pltpu.VMEM((nz, np_ * cap, width), jnp.bfloat16),
            DMA((2,)),
            DMA((nz,)),
            DMA((nz,)),
            DMA((nz,)),
            DMA((nz,)),
            DMA((nz,)),
            DMA((nz,)),
            DMA((nz, np_)),
            DMA((nz, np_)),
            DMA((nz, np_)),
            DMA((nz, np_)),
            DMA((nz,)),
        ],
        compiler_params=pltpu.CompilerParams(collective_id=1, has_side_effects=True),
        name="dispatch",
    )(part, residual, gain, picks, weights)


def combine_kernel(
    nz,
    np_,
    halves,
    weights,
    mixed,
    result,
    own_half,
    other_half,
    stage,
    back,
    sums,
    final,
    own_sem,
    core_send,
    core_recv,
    plane_send,
    plane_recv,
    col_send,
    col_recv,
):
    me, core, z, p, devices = partners(nz, np_)
    other = 1 - core
    cap = halves.shape[3]

    def load(d, k):
        return pltpu.make_async_copy(
            halves.at[p ^ k, z ^ d, core], own_half.at[p ^ k, z ^ d], own_sem.at[d, k]
        )

    def across(d, k):
        return push(
            halves.at[p ^ k, z ^ d, other],
            other_half.at[p ^ k, z ^ d],
            core_send.at[d, k],
            core_recv.at[d, k],
            me,
            other,
        )

    def slot(which):
        return pl.ds(pl.multiple_of(which * cap, cap), cap)

    def plane(d, k):
        q = p ^ k
        return push(
            stage.at[q, z ^ d],
            back.at[z ^ d, slot(p)],
            plane_send.at[d, k],
            plane_recv.at[d, k],
            z * np_ + q,
            core,
        )

    def plane_in(d, k):
        q = p ^ k
        return push(
            stage.at[q, z ^ d],
            back.at[z ^ d, slot(q)],
            plane_send.at[d, k],
            plane_recv.at[d, k],
            z * np_ + q,
            core,
        )

    def column(d):
        return push(
            sums.at[z ^ d],
            final.at[z],
            col_send.at[d],
            col_recv.at[d],
            (z ^ d) * np_ + p,
            core,
        )

    def column_in(d):
        return push(
            sums.at[z],
            final.at[z ^ d],
            col_send.at[d],
            col_recv.at[d],
            (z ^ d) * np_ + p,
            core,
        )

    def each(first, act):
        lax.fori_loop(first, np_, lambda k, c: (act(k), c)[1], 0)

    order = list(range(nz - 1, -1, -1))
    for d in order:
        each(0, lambda k: load(d, k).start())
    greet(devices)
    for d in order:
        each(0, lambda k: across(d, k).start())
    for d in order:

        def joined(k):
            load(d, k).wait()
            across(d, k).wait_recv()
            there = (p ^ k, z ^ d)
            return (
                own_half[there].astype(jnp.float32) + other_half[there].astype(jnp.float32)
            ).astype(jnp.bfloat16)

        def send_on(k):
            stage[p ^ k, z ^ d] = joined(k)
            plane(d, k).start()

        each(1, send_on)
        back[z ^ d, slot(p)] = joined(0)
    width = min(512, D)
    for d in order:
        each(1, lambda k: plane_in(d, k).wait_recv())
        there = z ^ d
        if d:
            for start in range(0, D, width):
                sums[there, :, start : start + width] = jnp.dot(
                    weights[there],
                    back[there, :, start : start + width],
                    preferred_element_type=jnp.float32,
                ).astype(jnp.bfloat16)
            column(d).start()
    for d in range(1, nz):
        column_in(d).wait_recv()
    for start in range(0, D, width):
        cols = slice(start, start + width)
        total = jnp.dot(weights[z], back[z, :, cols], preferred_element_type=jnp.float32)
        for d in range(1, nz):
            total = total + final[z ^ d, :, cols].astype(jnp.float32)
        result[:, cols] = (mixed[:, cols].astype(jnp.float32) + total).astype(jnp.bfloat16)
    for d in order:
        each(0, lambda k: across(d, k).wait_send())
        each(1, lambda k: plane(d, k).wait_send())
        if d:
            column(d).wait_send()


def combine(halves, weights, mixed):
    np_, nz, _, cap, width = halves.shape
    own_rows = mixed.shape[0]
    return pl.pallas_call(
        functools.partial(combine_kernel, nz, np_),
        out_shape=jax.ShapeDtypeStruct(mixed.shape, jnp.bfloat16),
        in_specs=[ANY, VMEM, VMEM],
        out_specs=VMEM,
        scratch_shapes=[
            pltpu.VMEM((np_, nz, cap, width), jnp.bfloat16),
            pltpu.VMEM((np_, nz, cap, width), jnp.bfloat16),
            pltpu.VMEM((np_, nz, cap, width), jnp.bfloat16),
            pltpu.VMEM((nz, np_ * cap, width), jnp.bfloat16),
            pltpu.VMEM((nz, own_rows, width), jnp.bfloat16),
            pltpu.VMEM((nz, own_rows, width), jnp.bfloat16),
            DMA((nz, np_)),
            DMA((nz, np_)),
            DMA((nz, np_)),
            DMA((nz, np_)),
            DMA((nz, np_)),
            DMA((nz,)),
            DMA((nz,)),
        ],
        compiler_params=pltpu.CompilerParams(collective_id=2, has_side_effects=True),
        name="combine",
    )(halves, weights, mixed)


def expert_act(row_block, gate_part, lin_part):
    gate_pre = jnp.dot(row_block, gate_part, preferred_element_type=jnp.float32)
    lin_pre = jnp.dot(row_block, lin_part, preferred_element_type=jnp.float32)
    gate_clip = jnp.minimum(gate_pre, CLAMP_LIMIT)
    lin_clip = jnp.clip(lin_pre, -CLAMP_LIMIT, CLAMP_LIMIT)
    return (gate_clip * jax.nn.sigmoid(SIGMOID_SLOPE * gate_clip) * (lin_clip + 1.0)).astype(
        jnp.bfloat16
    )


def local(
    queries,
    keys,
    values,
    out_gate,
    decay_rate,
    residual,
    out_weight,
    ffn_gain,
    route_ids,
    route_weights,
    gate_up,
    lin_up,
    down_weight,
):
    block_len = queries.shape[0]
    local_heads = decay_rate.shape[0]
    log_gamma = -decay_rate
    query_heads = queries.astype(jnp.float32).reshape(block_len, local_heads, DK).transpose(1, 0, 2)
    per_head_keys = keys.astype(jnp.float32).reshape(block_len, local_heads, DK).transpose(
        1, 0, 2
    ) * DK ** (-0.5)
    per_head_values = (
        values.astype(jnp.float32).reshape(block_len, local_heads, DV).transpose(1, 0, 2)
    )
    positions = jnp.arange(block_len, dtype=jnp.float32)
    offsets = positions[:, None] - positions[None, :]
    causal = offsets >= 0
    decay_mask = jnp.where(
        causal[None], jnp.exp(jnp.where(causal, offsets, 0.0)[None] * log_gamma[:, None, None]), 0.0
    )
    trailing_decay = jnp.exp((block_len - 1.0 - positions)[None, :] * log_gamma[:, None])
    lead_decay = jnp.exp((positions + 1.0)[None, :] * log_gamma[:, None])
    chain_decay = jnp.exp(block_len * log_gamma)
    attention_scores = (
        jnp.einsum("hqd,hkd->hqk", query_heads, per_head_keys, precision=TOP_PRECISION) * decay_mask
    )
    intra_block_term = jnp.einsum(
        "zfp,zpn->zfn", attention_scores, per_head_values, precision=TOP_PRECISION
    )
    state_delta = jnp.einsum(
        "mxs,mxq->msq",
        per_head_keys * trailing_decay[:, :, None],
        per_head_values,
        precision=TOP_PRECISION,
    )
    peers = lax.axis_size("sp")
    state_rows = local_heads * DK // peers
    head_of_row = (lax.axis_index("sp") * state_rows + jnp.arange(state_rows)) // DK
    row_decay = jnp.sum(
        jnp.where(head_of_row[:, None] == jnp.arange(local_heads)[None], chain_decay[None], 0.0),
        axis=1,
    )
    carried = (
        exchange_states(
            state_delta.astype(jnp.bfloat16).reshape(peers, state_rows, DV),
            jnp.broadcast_to(row_decay[:, None], (state_rows, DV)),
        )
        .reshape(local_heads, DK, DV)
        .astype(jnp.float32)
    )
    cross_term = (
        jnp.einsum("hqd,hdv->hqv", query_heads, carried, precision=TOP_PRECISION)
        * lead_decay[:, :, None]
    )
    retained = intra_block_term + cross_term
    normed = retained * lax.rsqrt(jnp.mean(retained * retained, axis=-1, keepdims=True) + EPS)
    gated = (
        normed.transpose(1, 0, 2).reshape(block_len, local_heads * DV)
        * jax.nn.silu(out_gate.astype(jnp.float32))
    ).astype(jnp.bfloat16)
    part = jnp.dot(gated, out_weight, preferred_element_type=jnp.float32).astype(jnp.bfloat16)
    own_rows, top_count = route_ids.shape
    capacity = own_rows * top_count * lax.axis_size("tp") // peers
    column = min(COLUMN, peers)
    plane = peers // column
    hits = route_ids[:, :, None] == jnp.arange(peers, dtype=jnp.int32)[None, None, :]
    named = jnp.any(hits, axis=1)
    weight_of = jnp.sum(jnp.where(hits, route_weights[:, :, None], 0.0), axis=1)
    earlier = jnp.arange(own_rows)[:, None] > jnp.arange(own_rows)[None, :]
    rank = jnp.dot(
        earlier.astype(jnp.bfloat16),
        named.astype(jnp.bfloat16),
        preferred_element_type=jnp.float32,
    ).astype(jnp.int32)
    slot_of = jnp.where(named, rank, -1)
    slots = jnp.arange(capacity, dtype=jnp.int32)
    picks = (slot_of.T[:, None, :] == slots[None, :, None]).astype(jnp.bfloat16)
    picks = picks.reshape(column, plane * capacity, own_rows)
    weights = jnp.where(
        slot_of.reshape(own_rows, column, plane).transpose(1, 0, 2)[:, :, :, None] == slots,
        weight_of.reshape(own_rows, column, plane).transpose(1, 0, 2)[:, :, :, None],
        0.0,
    ).astype(jnp.bfloat16)
    weights = weights.reshape(column, own_rows, plane * capacity)
    mixed, landed, weights_in = dispatch(
        part, residual, ffn_gain[None, :], picks, weights, plane, capacity
    )
    activation = expert_act(landed.reshape(-1, D), gate_up[0], lin_up[0])
    halves = (
        jnp.dot(activation, down_weight[0], preferred_element_type=jnp.float32)
        .astype(jnp.bfloat16)
        .reshape(landed.shape)
    )
    return combine(halves, weights_in, mixed)


def solution(mesh):
    placed = (
        P("sp", "tp"),
        P("sp", "tp"),
        P("sp", "tp"),
        P("sp", "tp"),
        P("tp"),
        P(("sp", "tp"), None),
        P("tp", None),
        P(),
        P(("sp", "tp"), None),
        P(("sp", "tp"), None),
        P("sp", None, "tp"),
        P("sp", None, "tp"),
        P("sp", "tp", None),
    )
    return jax.shard_map(
        local, mesh=mesh, in_specs=placed, out_specs=P(("sp", "tp"), None), check_vma=False
    )
```

time: 293 us -> 141 us (0.48); the launches traced: 288 us -> 141 us
  Pallas kernels: 0 us -> 105 us
  waiting for transfers between devices: 102 us -> 0 us
  blocking collectives: 99.8 us -> 0 us
  other arithmetic: 26 us -> 4.21 us
  between operations: 14.1 us -> 0.23 us
  local copies, waits for them, and re-layouts: 12 us -> 4.09 us
  starting transfers between devices: 7.21 us -> 0 us
    pallas_call x0 -> x3, Pallas kernels: none -> 105 us  [the longest x1 42.8 us: dispatch(): pl.pallas_call(functools.partial(dispatch_kernel, nz, np_), out_shape=(ja...]
    all_to_all x1 -> x0, blocking collectives: 55.8 us -> none  [local(): lax.all_to_all(outgoing, 'sp', split_axis=0, concat_axis=0, tiled=True)]
    unnamed x1 -> x0, blocking collectives: 43.9 us -> none
    all_to_all x1 -> x0, waiting for transfers between devices: 42.5 us -> none  [local(): lax.all_to_all(summed, 'sp', split_axis=0, concat_axis=0, tiled=True)]
    all_gather x2 -> x0, waiting for transfers between devices: 41.2 us -> none  [the longest x1 29.2 us: entering(): lax.all_gather(part.astype(kind), axis)]
    reduce_scatter x2 -> x0, waiting for transfers between devices: 17.9 us -> none  [the longest x1 13.4 us: local(): lax.psum_scatter(partial_value.astype(jnp.bfloat16), 'tp', scatter_dimens...]
    select_n x19 -> x1, other arithmetic: 17.5 us -> 0.01 us  [local(): (lax.axis_index('sp') * state_rows + jnp.arange(state_rows)) // DK]
    all_to_all x1 -> x0, starting transfers between devices: 6.9 us -> none  [local(): lax.all_to_all(summed, 'sp', split_axis=0, concat_axis=0, tiled=True)]
  transfers between devices with their start and end apart: 5 -> 0, of which waited for: 5 -> 0; matrix products, arithmetic and copies ran while one was open for 3% -> 0% of each run, Pallas kernels for 0% -> 0%
where the time goes in v1:
time: 141 us
  Pallas kernels  105 us (74%)
  matrix products  27.4 us (19%)
  other arithmetic  4.21 us (3%)
  local copies, waits for them, and re-layouts  4.09 us (3%)
    pallas_call x1, Pallas kernels, dispatch(): pl.pallas_call(functools.partial(dispatch_kernel, nz, np_), out_shape=(ja...  42.8 us
    pallas_call x1, Pallas kernels, combine(): pl.pallas_call(functools.partial(combine_kernel, nz, np_), out_shape=jax....  39.9 us
    pallas_call x1, Pallas kernels, exchange_states(): pl.pallas_call(functools.partial(state_kernel, n), out_shape=jax.ShapeDty...  22.1 us
    dot_general x1, matrix products, expert_act(): lin_pre = jnp.dot(row_block, lin_part, preferred_element_type=jnp.float32)  7.66 us
    dot_general x1, matrix products, local(): jnp.dot(activation, down_weight[0], preferred_element_type=jnp.float32)  6.07 us
    dot_general x1, matrix products, expert_act(): gate_pre = jnp.dot(row_block, gate_part, preferred_element_type=jnp.float32)  5.75 us
    dot_general x1, matrix products, local(): jnp.dot(gated, out_weight, preferred_element_type=jnp.float32)  3.73 us

profile of v1, /device:TPU:0, one launch (start us, length us, event | category | flops | bytes accessed | tf_op | source)
XLA Modules:
  0.0 140.8 jit_solution(4482061471721350090)
XLA Ops:
  0.0 0.0 copy-start
  0.0 0.0 copy-start.2
  0.0 0.0 copy-start.1
  0.0 0.7 multiply_exponential_fusion.2
  0.7 0.1 select_reduce_fusion.1
  0.8 0.1 multiply_exponential_fusion.1
  0.9 0.7 fusion.35
  1.6 0.1 eq.75
  1.7 0.1 multiply_exponential_fusion
  1.8 0.7 select_reduce_fusion
  2.5 0.1 fusion.12
  2.7 0.7 broadcast_in_dim.60.decay
  3.4 0.1 copy.46
  3.5 0.7 fusion.25.picks
  4.3 0.1 copy.45
  4.4 0.6 select_convert_fusion.weights
  5.1 1.0 copy.51
  6.1 0.0 copy-done
  6.1 0.4 fusion.11
  6.5 2.0 %convolution_convert_fusion.1 = bf16[4,128,256]{2,1,0:T(8,128)(2,1)} fusion(f32[4,128,128]{1,2,0:T(8,128)S(1)} %bitcast.97, bf16[16,4,8,256]{3,2,1,0:T(8,128)(2,1)} %bitcast.100, f32[4,128]{1,0:T(4,128)S(1)} %get-tuple-element.12), kind=kOutput, calls=%fused_computation.9 | convolution fusion | flops 201523200 | bytes 788480 | tf_op jit(solution)/shard_map/mxs,mxq->msq/dot_general | solution.py:530
  8.5 22.1 %states.1 = bf16[16,32,256]{2,1,0:T(8,128)(2,1)} custom-call(bf16[16,32,256]{2,1,0:T(8,128)(2,1)} %bitcast.98, f32[32,256]{1,0:T(8,128)} %broadcast_in_dim.60.decay), custom_call_target="tpu_custom_call" | custom-call | tf_op jit(solution)/shard_map/states/pallas_call | solution.py:88
  30.6 1.2 fusion.28
  31.8 0.0 copy-done.2
  31.8 0.2 copy.44
  32.0 0.0 copy-done.1
  32.0 0.5 fusion.18
  32.5 0.2 fusion.20
  32.8 0.2 copy.43
  33.0 0.2 fusion.21
  33.1 3.7 %convolution_convert_fusion.part = bf16[128,2048]{1,0:T(8,128)(2,1)} fusion(bf16[128,1024]{0,1:T(8,128)(2,1)S(1)} %fusion.21, bf16[1024,2048]{1,0:T(8,128)(2,1)} %param.19), kind=kOutput, calls=%fused_computation.8 | convolution fusion | flops 537133056 | bytes 4980736 | tf_op jit(solution)/shard_map/dot_general | solution.py:561
  36.8 42.8 %dispatch.1 = (bf16[64,2048]{1,0:T(8,128)(2,1)}, bf16[4,4,2,32,2048]{4,3,2,1,0:T(8,128)(2,1)}, bf16[4,64,128]{2,1,0:T(8,128)(2,1)}) custom-call(bf16[128,2048]{1,0:T(8,128)(2,1)} %convolution_convert_fusion.part, bf16[64,2048]{1,0:T(8,128)(2,1)} %residual.1, f32[1,2048]{1,0:T(1,128)} %bitcast.108, bf16[4,128,64]{2,1,0:T(8,128)(2,1)} %fusion.25.picks, ...), custom_call_target="tpu_custom_call" | custom-call | tf_op jit(solution)/shard_map/dispatch/pallas_call | solution.py:283
  79.7 0.0 copy-start.3
  79.7 0.0 copy-start.5
  79.7 7.7 %fusion.2 = f32[1024,1024]{1,0:T(8,128)S(1)} fusion(bf16[1024,2048]{1,0:T(8,128)(2,1)} %bitcast.109, bf16[1,2048,1024]{2,1,0:T(8,128)(2,1)} %param.24), kind=kOutput, calls=%fused_computation.2 | convolution fusion | flops 4294967296 | bytes 12582912 | tf_op jit(solution)/shard_map/dot_general | solution.py:482
  87.4 0.0 copy-done.3
  87.4 0.0 copy-done.5
  87.4 0.0 copy-start.4
  87.4 5.7 %multiply_convert_fusion = bf16[1024,1024]{1,0:T(8,128)(2,1)S(1)} fusion(f32[1024,1024]{1,0:T(8,128)S(1)} %fusion.2, bf16[1024,2048]{1,0:T(8,128)(2,1)S(1)} %bitcast.110, bf16[1,2048,1024]{2,1,0:T(8,128)(2,1)S(1)} %copy-done.3), kind=kOutput, calls=%fused_computation.6 | convolution fusion | flops 4305453056 | bytes 14680064 | tf_op jit(solution)/shard_map/dot_general | solution.py:481
  93.1 0.0 copy-done.4
  93.2 6.1 %fusion.6 = bf16[1024,2048]{1,0:T(8,128)(2,1)} fusion(bf16[1024,1024]{1,0:T(8,128)(2,1)S(1)} %multiply_convert_fusion, bf16[1,1024,2048]{2,1,0:T(8,128)(2,1)S(1)} %copy-done.4), kind=kOutput, calls=%fused_computation.7 | convolution fusion | flops 4297064448 | bytes 10485760 | tf_op jit(solution)/shard_map/dot_general | solution.py:590
  99.2 39.9 %combine.1 = bf16[64,2048]{1,0:T(8,128)(2,1)} custom-call(bf16[4,4,2,32,2048]{4,3,2,1,0:T(8,128)(2,1)} %bitcast.95, bf16[4,64,128]{2,1,0:T(8,128)(2,1)} %get-tuple-element.9.weights, bf16[64,2048]{1,0:T(8,128)(2,1)} %get-tuple-element.10.mixed), custom_call_target="tpu_custom_call" | custom-call | tf_op jit(solution)/shard_map/combine/pallas_call | solution.py:455
  139.2 1.7 %copy.73 = bf16[64,2048]{1,0:T(8,128)(2,1)} copy(bf16[64,2048]{1,0:T(8,128)(2,1)} %combine.1) | data formatting | bytes 524288
  (9 shorter events, 0.1 us)
Async XLA Ops:
  0.0 6.1 %copy-start = (bf16[128,512]{1,0:T(8,128)(2,1)S(1)}, bf16[128,512]{1,0:T(8,128)(2,1)}, u32[]{:S(2)}) copy-start(bf16[128,512]{1,0:T(8,128)(2,1)} %param.13) | copy-start | bytes 393220
  0.0 31.8 %copy-start.2 = (bf16[128,1024]{1,0:T(8,128)(2,1)S(1)}, bf16[128,1024]{1,0:T(8,128)(2,1)}, u32[]{:S(2)}) copy-start(bf16[128,1024]{1,0:T(8,128)(2,1)} %param.16) | copy-start | bytes 786436
  0.0 32.0 %copy-start.1 = (bf16[128,1024]{1,0:T(8,128)(2,1)S(1)}, bf16[128,1024]{1,0:T(8,128)(2,1)}, u32[]{:S(2)}) copy-start(bf16[128,1024]{1,0:T(8,128)(2,1)} %param.15) | copy-start | bytes 786436
  79.7 7.7 %copy-start.3 = (bf16[1,2048,1024]{2,1,0:T(8,128)(2,1)S(1)}, bf16[1,2048,1024]{2,1,0:T(8,128)(2,1)}, u32[]{:S(2)}) copy-start(bf16[1,2048,1024]{2,1,0:T(8,128)(2,1)} %param.23) | copy-start | bytes 12582916
  79.7 7.7 %copy-start.5 = (bf16[4,4,2,32,2048]{4,3,2,1,0:T(8,128)(2,1)S(1)}, bf16[4,4,2,32,2048]{4,3,2,1,0:T(8,128)(2,1)}, u32[]{:S(2)}) copy-start(bf16[4,4,2,32,2048]{4,3,2,1,0:T(8,128)(2,1)} %get-tuple-element.8) | copy-start | bytes 12582916
  87.4 5.8 %copy-start.4 = (bf16[1,1024,2048]{2,1,0:T(8,128)(2,1)S(1)}, bf16[1,1024,2048]{2,1,0:T(8,128)(2,1)}, u32[]{:S(2)}) copy-start(bf16[1,1024,2048]{2,1,0:T(8,128)(2,1)} %param.25) | copy-start | bytes 12582916
